TPU v7x, 32 devices: a whole 2x2x4 slice. The times are simulated.
32 devices in a mesh: sp: 8 (over z, y), tp: 4 (over x, core).
Axes of the slice: x: 2, y: 2, z: 4, core: 2. Of those that a mesh axis runs over, the one named last changes fastest.
Arguments:
- tokens: bfloat16 [2048, 2048], P('sp', 'tp'), may hold values from -19 to 250
- in_gain: bfloat16 [2048], replicated, may hold values from 0.099609375 to 1.8984375
- w_glu_value: bfloat16 [2048, 512], P(None, 'tp'), may hold values from -0.125 to 0.125
- w_glu_gate: bfloat16 [2048, 512], P(None, 'tp'), may hold values from -0.125 to 0.125
- w_query: bfloat16 [2048, 1024], P(None, 'tp'), may hold values from -1 to 1
- w_key: bfloat16 [2048, 512], P(None, 'tp'), may hold values from -1 to 1
- w_value: bfloat16 [2048, 512], P(None, 'tp'), may hold values from -0.125 to 0.125
- w_gate_conv: bfloat16 [2048, 512], P(None, 'tp'), may hold values from -0.125 to 0.125
- w_gate_attn: bfloat16 [2048, 1024], P(None, 'tp'), may hold values from -0.125 to 0.125
- conv_weight: bfloat16 [31, 512], P(None, 'tp'), may hold values from -4.6 to 4.6
- conv_gain: float32 [512], P('tp'), may hold values from 0.1 to 1.9
- lam: float32 [8], P('tp'), may hold values from 0.3 to 0.8
- head_gain: float32 [128], replicated, may hold values from 0.1 to 1.9
- out_conv: bfloat16 [512, 2048], P('tp'), may hold values from -0.15625 to 0.15625
- out_attn: bfloat16 [1024, 2048], P('tp'), may hold values from -0.15625 to 0.15625
Outputs:
- mixed: bfloat16 [2048, 2048], P(('sp', 'tp'))
All inputs are finite; a program needn't handle non-finite values.
Results may differ from a plain program's by a relative error of at most 0.017.
The roundings to bfloat16 on the way count: a program that leaves them out, or rounds other values in their place, can miss the bound.
Values may be sent and summed in bfloat16 or wider, within the bound.
A program may use at most 128 MiB of HBM per device.

v0:
```python
import math
import jax
import jax.numpy as jnp
from jax import lax
from jax.sharding import PartitionSpec as P

D = 2048
CONV = 512
QK = 64
VDIM = 128
WIDTH = 31
EPSILON = 1e-06
NEG_BIG = -1e30
HEAD_SCALE = 0.8


def shifted(x, axis, by):
    count = lax.axis_size(axis)
    pairs = [(i, i + by) for i in range(count) if 0 <= i + by < count]
    return lax.ppermute(x, axis, pairs)


def local(
    tokens,
    in_gain,
    w_glu_value,
    w_glu_gate,
    w_query,
    w_key,
    w_value,
    w_gate_conv,
    w_gate_attn,
    conv_weight,
    conv_gain,
    lam,
    head_gain,
    out_conv,
    out_attn,
):
    tok_rows = tokens.shape[0]
    weights = (w_glu_value, w_glu_gate, w_query, w_key, w_value, w_gate_conv, w_gate_attn)
    widened = lax.all_gather(tokens, "tp", axis=1, tiled=True).astype(jnp.float32)
    gain_part = in_gain.astype(jnp.float32)
    scaled = (widened * gain_part[None, :]).astype(jnp.bfloat16)
    updated = tuple(
        (jnp.dot(scaled, weight, preferred_element_type=jnp.float32) for weight in weights)
    )
    squares = jnp.sum(widened * widened, axis=1)
    inv_rms = lax.rsqrt(squares / D + EPSILON)[:, None]
    glu_value, glu_gate, query, key, value, gate_conv, gate_attn = [
        (total * inv_rms).astype(jnp.bfloat16) for total in updated
    ]
    glued = (glu_value.astype(jnp.float32) * jax.nn.sigmoid(glu_gate.astype(jnp.float32))).astype(
        jnp.bfloat16
    )
    tail_rows = WIDTH - 1
    last_rows = glued[tok_rows - tail_rows :]
    conv_local = glued.shape[1]
    kv_local = key.shape[1] // (2 * QK)
    heads_local = lam.shape[0]
    group = heads_local // kv_local
    my_index = lax.axis_index("sp")
    my_start = my_index * tok_rows
    scale_factor = 1.0 / math.sqrt(QK)
    query_groups = [
        (
            query.reshape(tok_rows, kv_local, group, 2, QK),
            my_start + jnp.arange(tok_rows, dtype=jnp.int32),
        )
    ]
    start_attn = tuple(
        (
            (
                jnp.full((kv_local, group, 2, rows_of.shape[0]), NEG_BIG, jnp.float32),
                jnp.zeros((kv_local, group, 2, rows_of.shape[0]), jnp.float32),
                jnp.zeros((kv_local, group, 2, rows_of.shape[0], VDIM), jnp.float32),
            )
            for rows_of, unused_pos in query_groups
        )
    )
    key_piece = lax.all_gather(key, "sp", axis=0, tiled=True)
    value_piece = lax.all_gather(value, "sp", axis=0, tiled=True)
    shards = key_piece.shape[0] // tok_rows
    stacked_keys = key_piece.reshape(shards, tok_rows, kv_local, 2, QK)
    stacked_values = value_piece.reshape(shards, tok_rows, kv_local, VDIM)
    firsts = tok_rows * jnp.arange(shards, dtype=jnp.int32)

    def visit(states, inputs):
        key_shard, value_shard, first = inputs
        key_pos = first + jnp.arange(tok_rows, dtype=jnp.int32)
        updated_states = []
        for (query_rows, query_pos), current_state in zip(query_groups, states):

            def update(current, query_rows=query_rows, query_pos=query_pos):
                maxima, totals, summed = current
                scores = (
                    jnp.einsum(
                        "qagcd,kacd->agcqk",
                        query_rows,
                        key_shard,
                        preferred_element_type=jnp.float32,
                    )
                    * scale_factor
                )
                allowed = key_pos[None, :] <= query_pos[:, None]
                scores = jnp.where(allowed, scores, NEG_BIG)
                new_max = jnp.maximum(maxima, jnp.max(scores, axis=4))
                factor = jnp.exp(maxima - new_max)
                expd = jnp.exp(scores - new_max[..., None])
                totals = totals * factor + jnp.sum(expd, axis=4)
                summed = summed * factor[..., None] + jnp.einsum(
                    "agcqk,kav->agcqv",
                    expd.astype(jnp.bfloat16),
                    value_shard,
                    preferred_element_type=jnp.float32,
                )
                return (new_max, totals, summed)

            def keep(current):
                return current

            query_last = query_pos[0] + query_pos.shape[0] - 1
            updated_states.append(lax.cond(first <= query_last, update, keep, current_state))
        return (tuple(updated_states), None)

    result, unused = lax.scan(visit, start_attn, (stacked_keys, stacked_values, firsts))
    states = result
    maxima, totals, summed = states[0]
    output = (
        summed[:, :, 0] / totals[:, :, 0][..., None]
        - lam.reshape(kv_local, group)[:, :, None, None]
        * summed[:, :, 1]
        / totals[:, :, 1][..., None]
    )
    normed = output * lax.rsqrt(jnp.mean(output * output, axis=3, keepdims=True) + EPSILON)
    normed = normed * head_gain[None, None, None, :] * HEAD_SCALE
    laid = jnp.transpose(normed, (2, 0, 1, 3)).reshape(normed.shape[2], heads_local * VDIM)
    y_attn = (laid * jax.nn.silu(gate_attn.astype(jnp.float32))).astype(jnp.bfloat16)
    previous = shifted(last_rows, "sp", 1)
    padded = jnp.concatenate([previous, glued], axis=0).astype(jnp.float32)
    taps = conv_weight.astype(jnp.float32)
    conv = jnp.zeros((tok_rows, conv_local), jnp.float32)
    for offset in range(WIDTH):
        conv = conv + padded[offset : offset + tok_rows] * taps[offset][None, :]
    total_sq = lax.psum(jnp.sum(conv * conv, axis=1), "tp")
    normed = conv * lax.rsqrt(total_sq / CONV + EPSILON)[:, None] * conv_gain[None, :]
    y_conv = (jax.nn.silu(normed) * jax.nn.silu(gate_conv.astype(jnp.float32))).astype(jnp.bfloat16)
    return lax.psum_scatter(
        (
            jnp.dot(y_conv, out_conv, preferred_element_type=jnp.float32)
            + jnp.dot(y_attn, out_attn, preferred_element_type=jnp.float32)
        ).astype(jnp.bfloat16),
        "tp",
        scatter_dimension=0,
        tiled=True,
    )


def solution(mesh):
    in_specs = (
        P("sp", "tp"),
        P(),
        P(None, "tp"),
        P(None, "tp"),
        P(None, "tp"),
        P(None, "tp"),
        P(None, "tp"),
        P(None, "tp"),
        P(None, "tp"),
        P(None, "tp"),
        P("tp"),
        P("tp"),
        P(),
        P("tp", None),
        P("tp", None),
    )
    out_specs = P(("sp", "tp"), None)
    return jax.shard_map(local, mesh=mesh, in_specs=in_specs, out_specs=out_specs, check_vma=False)
```

profile of v0, /device:TPU:0, one launch (start us, length us, event | category | flops | bytes accessed | tf_op | source)
XLA Modules:
  0.0 186.6 jit_solution(6918326451705439415)
XLA Ops:
  6.5 0.0 copy-start
  6.5 0.0 all-gather.2.cloned.1.call-start
  6.5 0.7 all-gather.2.cloned.1.call-update
  7.3 0.0 reduce-scatter.2.cloned.1.call-start
  7.3 0.7 convert_element_type.71
  8.0 0.5 slice.269
  8.5 0.7 convert_element_type.79
  9.8 18.6 %all-gather.2.cloned.1.call-done = bf16[256,2048]{1,0:T(8,128)(2,1)} async-done(((bf16[256,512]{1,0:T(8,128)(2,1)}), bf16[256,2048]{1,0:T(8,128)(2,1)}) %all-gather.2.cloned.1.call-update) | async-done | bytes 1048592 | tf_op jit(solution)/shard_map/all_gather | solution.py:42
  28.3 1.5 fusion.19
  29.9 1.8 fusion.35
  31.7 0.0 copy-start.1
  31.7 33.5 %all_gather.10 = bf16[2048,128]{1,0:T(8,128)(2,1)} all-gather(bf16[256,128]{1,0:T(8,128)(2,1)S(1)} %fusion.35), channel_id=1, replica_groups=mesh['sp'=8,'tp'=4] {'sp'}, dimensions={0}, use_global_device_ids=true | all-gather | bytes 589824 | tf_op jit(solution)/shard_map/all_gather | solution.py:81
  65.2 2.4 %reshape.159 = bf16[8,256,1,2,64]{4,3,1,0,2:T(2,128)(2,1)S(1)} reshape(bf16[2048,128]{1,0:T(8,128)(2,1)} %all_gather.10) | data formatting | bytes 1048576 | tf_op jit(solution)/shard_map/reshape | solution.py:84
  67.6 1.8 copy.27
  69.4 0.0 copy-done.1
  69.4 0.0 copy-start.5
  69.4 1.6 fusion.36
  70.9 31.3 %all_gather.11 = bf16[2048,128]{1,0:T(8,128)(2,1)S(1)} all-gather(bf16[256,128]{1,0:T(8,128)(2,1)S(1)} %fusion.36), channel_id=1, replica_groups=mesh['sp'=8,'tp'=4] {'sp'}, dimensions={0}, use_global_device_ids=true | all-gather | bytes 589824 | tf_op jit(solution)/shard_map/all_gather | solution.py:82
  102.2 0.0 copy-done.5
  102.2 0.6 fusion.20
  102.9 0.0 copy-start.4
  102.9 0.0 copy-start.2
  102.9 13.8 %while.17 = (s32[]{:T(128)}, f32[1,2,2,256]{3,1,2,0:T(2,128)S(1)}, f32[1,2,2,256]{3,1,2,0:T(2,128)S(1)}, f32[1,2,2,256,128]{4,3,2,1,0:T(8,128)S(1)}, s32[8]{0:T(...) while((s32[]{:T(128)}, f32[1,2,2,256]{3,1,2,0:T(2,128)S(1)}, ...), condition=%wide.region_8.9_spmd.clone, body=%wide.region_3.8_spmd.clone.sunk | while | flops 102567424 | bytes 4665123 | solution.py:126
  102.9 0.7 dynamic_slice.38
  104.3 2.8 %conditional.3 = ((f32[1,2,2,256]{3,1,2,0:T(2,128)S(1)}, f32[1,2,2,256]{3,1,2,0:T(2,128)S(1)}, f32[1,2,2,256,128]{4,3,2,1,0:T(8,128)S(1)})) conditional(s32[]{:T(128)} %convert_element_type.190, (f32[1,2,2,256]{3,1,2,0:T(2,128)S(1)}, f32[1,2,2,256]{3,1,2,0:T(2,128)S(1)}, f32[1,2,2,256,128]{4,3,2,1,0:T(8,128)S(1)}) %tuple.82, (s32[]{:T(128)}, ...), branch_computations={%region_4.4_spmd, %region_5.7_spmd} | conditional | flops 102567424 | bytes 4663852 | solution.py:123
  104.3 0.7 broadcast_add_fusion
  105.0 0.1 broadcast_compare_fusion
  105.1 1.2 fusion.99
  106.3 0.2 fusion.7
  106.5 0.5 fusion.4
  107.1 0.7 dynamic_slice.38
  108.5 0.7 dynamic_slice.38
  109.8 0.7 dynamic_slice.38
  111.2 0.7 dynamic_slice.38
  112.6 0.7 dynamic_slice.38
  114.0 0.7 dynamic_slice.38
  115.3 0.7 dynamic_slice.38
  116.7 0.0 copy-done.4
  116.7 0.0 copy-start.7
  116.7 0.3 multiply_reduce_fusion
  117.1 0.0 copy-done.2
  117.1 0.1 multiply_bitcast_fusion
  117.2 0.1 copy.31
  117.4 0.0 copy-start.6
  117.4 1.6 fusion.32
  119.0 0.0 copy-done.7
  119.0 0.4 fusion.26
  119.4 6.5 %collective-permute-start = (bf16[30,128]{1,0:T(8,128)(2,1)S(1)}, bf16[30,128]{1,0:T(8,128)(2,1)S(1)}, u32[]{:S(2)}, u32[]{:S(2)}) collective-permute-start(bf16[30,128]{1,0:T(8,128)(2,1)S(1)} %slice.274), channel_id=1, source_target_pairs={{0,4},{4,8},{8,12},{12,16},{16,20},{20,24},{24,28},{1,5},{5,9},{9,... | collective-permute-start | bytes 23048 | tf_op jit(solution)/shard_map/ppermute | solution.py:20
  125.9 0.0 copy-done.6
  125.9 0.6 fusion.47
  126.5 0.7 collective-permute-done
  127.3 0.0 copy-start.3
  127.3 0.6 multiply_reduce_fusion.1
  127.9 5.8 %psum.7 = f32[256]{0:T(256)S(1)} all-reduce(f32[256]{0:T(256)S(1)} %get-tuple-element.287), channel_id=1, replica_groups=mesh['sp'=8,'tp'=4] {'tp'}, use_global_device_ids=true, to_apply=%region_2.3 | all-reduce | flops 256 | bytes 2048 | tf_op jit(solution)/shard_map/psum | solution.py:145
  133.7 0.0 copy-done.3
  133.7 2.3 %fusion.83 = f32[256,2048]{1,0:T(8,128)S(1)} fusion(bf16[128,2048]{1,0:T(8,128)(2,1)} %param.32, bf16[2048,128]{1,0:T(8,128)(2,1)} %param.26, bf16[256,2048]{1,0:T(8,128)(2,1)} %all-gather.2.cloned.1.call-done, f32[2048]{0:T(1024)S(1)} %convert_element_type.71, f32[256,128]{1,0:T(8,128)S(1)} %get-tuple-element.288, f32[128]{0:T(128)S(1)} %copy-done.3, ...), kind=kOutput, calls=%fused_computation.126 | convolution fusion | flops 270499840 | bytes 4336128 | tf_op jit(solution)/shard_map/dot_general | solution.py:150
  136.0 0.0 copy-done
  136.0 1.4 fusion.17
  137.4 0.0 reduce-scatter.2.cloned.1.call-update
  137.4 42.3 %reduce-scatter.2.cloned.1.call-done = bf16[64,2048]{1,0:T(8,128)(2,1)} async-done(((bf16[256,2048]{1,0:T(8,128)(2,1)}), bf16[64,2048]{1,0:T(8,128)(2,1)}) %reduce-scatter.2.cloned.1.call-update) | async-done | bytes 262160 | tf_op jit(solution)/shard_map/reduce_scatter | solution.py:148
  (33 shorter events, 0.3 us)
Async XLA Ops:
  6.5 129.4 %copy-start = (bf16[256,2048]{1,0:T(8,128)(2,1)S(1)}, bf16[256,2048]{1,0:T(8,128)(2,1)}, u32[]{:S(2)}) copy-start(bf16[256,2048]{1,0:T(8,128)(2,1)} %param.33) | copy-start | bytes 3145732
  6.5 21.8 %all-gather.2.cloned.1.call-start = ((), (), s32[]{:S(2)}) async-start(), calls=%async_computation.1 | async-start | bytes 1310720 | tf_op jit(solution)/shard_map/all_gather | solution.py:42
  7.3 172.5 %reduce-scatter.2.cloned.1.call-start = ((), (), s32[]{:S(2)}) async-start(), calls=%async_computation.2 | async-start | bytes 1310720 | tf_op jit(solution)/shard_map/reduce_scatter | solution.py:148
  31.7 37.7 %copy-start.1 = (bf16[256,2048]{1,0:T(8,128)(2,1)S(1)}, bf16[256,2048]{1,0:T(8,128)(2,1)}, u32[]{:S(2)}) copy-start(bf16[256,2048]{1,0:T(8,128)(2,1)} %all-gather.2.cloned.1.call-done) | copy-start | bytes 3145732
  69.4 32.8 %copy-start.5 = (bf16[2048,256]{1,0:T(8,128)(2,1)S(1)}, bf16[2048,256]{1,0:T(8,128)(2,1)}, u32[]{:S(2)}) copy-start(bf16[2048,256]{1,0:T(8,128)(2,1)} %param.23) | copy-start | bytes 3145732
  102.9 13.8 %copy-start.4 = (f32[2]{0:T(128)S(1)}, f32[2]{0:T(128)}, u32[]{:S(2)}) copy-start(f32[2]{0:T(128)} %param.30) | copy-start | bytes 28
  102.9 14.2 %copy-start.2 = (f32[128]{0:T(128)S(1)}, f32[128]{0:T(128)}, u32[]{:S(2)}) copy-start(f32[128]{0:T(128)} %param.31) | copy-start | bytes 1540
  116.7 2.2 %copy-start.7 = (bf16[2048,128]{1,0:T(8,128)(2,1)S(1)}, bf16[2048,128]{1,0:T(8,128)(2,1)}, u32[]{:S(2)}) copy-start(bf16[2048,128]{1,0:T(8,128)(2,1)} %param.21) | copy-start | bytes 1572868
  117.4 8.5 %copy-start.6 = (bf16[2048,256]{1,0:T(8,128)(2,1)S(1)}, bf16[2048,256]{1,0:T(8,128)(2,1)}, u32[]{:S(2)}) copy-start(bf16[2048,256]{1,0:T(8,128)(2,1)} %param.27) | copy-start | bytes 3145732
  119.4 7.8 %collective-permute-start = (bf16[30,128]{1,0:T(8,128)(2,1)S(1)}, bf16[30,128]{1,0:T(8,128)(2,1)S(1)}, u32[]{:S(2)}, u32[]{:S(2)}) collective-permute-start(bf16[30,128]{1,0:T(8,128)(2,1)S(1)} %slice.274), channel_id=1, source_target_pairs={{0,4},{4,8},{8,12},{12,16},{16,20},{20,24},{24,28},{1,5},{5,9},{9,... | collective-permute-start | bytes 23048 | tf_op jit(solution)/shard_map/ppermute | solution.py:20
  127.3 6.4 %copy-start.3 = (f32[128]{0:T(128)S(1)}, f32[128]{0:T(128)}, u32[]{:S(2)}) copy-start(f32[128]{0:T(128)} %param.29) | copy-start | bytes 1540
Sparse Core Ops, SparseCore 0:
  8.9 19.4 all-gather.1
  137.6 42.1 reduce-scatter.1
where the time goes:
time: 187 us
  blocking collectives  70.6 us (38%)
  waiting for transfers between devices  62.3 us (33%)
  between operations  14.2 us (8%)
  matrix products  12 us (6%)
  local copies, waits for them, and re-layouts  10.2 us (5%)
  starting transfers between devices  6.53 us (3%)
  loops' own time  5.83 us (3%)
  other arithmetic  4.96 us (3%)
    reduce_scatter x1, waiting for transfers between devices, local(): lax.psum_scatter((jnp.dot(y_conv, out_conv, preferred_element_type=jnp.fl...  42.3 us
    all_gather x1, blocking collectives, local(): key_piece = lax.all_gather(key, 'sp', axis=0, tiled=True)  33.5 us
    all_gather x1, blocking collectives, local(): value_piece = lax.all_gather(value, 'sp', axis=0, tiled=True)  31.3 us
    all_gather x1, waiting for transfers between devices, local(): lax.all_gather(tokens, 'tp', axis=1, tiled=True).astype(jnp.float32)  18.6 us
    dot_general x6, matrix products, local(): jnp.dot(scaled, weight, preferred_element_type=jnp.float32)  6.52 us
    ppermute x1, starting transfers between devices, shifted(): return lax.ppermute(x, axis, pairs)  6.49 us
    psum x1, blocking collectives, local(): total_sq = lax.psum(jnp.sum(conv * conv, axis=1), 'tp')  5.8 us
    another operation x1, loops' own time, local(): lax.scan(visit, start_attn, (stacked_keys, stacked_values, firsts))  5.67 us
  transfers between devices with their start and end apart: 3, of which 3 were waited for; matrix products, arithmetic and copies ran while one was open for 1% of the time, Pallas kernels for 0%

commit v1 on v0

--- a/solution.py
+++ b/solution.py
@@ -39,7 +39,7 @@
 ):
     tok_rows = tokens.shape[0]
     weights = (w_glu_value, w_glu_gate, w_query, w_key, w_value, w_gate_conv, w_gate_attn)
-    widened = lax.all_gather(tokens, "tp", axis=1, tiled=True).astype(jnp.float32)
+    widened = jnp.concatenate(lax.all_gather(tokens, "tp"), axis=1).astype(jnp.float32)
     gain_part = in_gain.astype(jnp.float32)
     scaled = (widened * gain_part[None, :]).astype(jnp.bfloat16)
     updated = tuple(

time: 187 us -> 200 us (1.070)
  other arithmetic: 4.96 us -> 9.77 us
  waiting for transfers between devices: 62.3 us -> 66.5 us
  local copies, waits for them, and re-layouts: 10.2 us -> 14.1 us
  starting transfers between devices: 6.53 us -> 3.42 us
  blocking collectives: 70.6 us -> 72.7 us
    reduce_scatter x1, waiting for transfers between devices: 42.3 us -> 48 us  [local(): lax.psum_scatter((jnp.dot(y_conv, out_conv, preferred_element_type=jnp.fl...]
    convert_element_type x0 -> x2, other arithmetic: none -> 4.86 us  [the longest x1 2.85 us: local(): jnp.concatenate(lax.all_gather(tokens, 'tp'), axis=1).astype(jnp.float32)]
    ppermute x1, starting transfers between devices: 6.49 us -> 3.38 us  [shifted(): return lax.ppermute(x, axis, pairs)]
    convert_element_type x0 -> x1, local copies, waits for them, and re-layouts: none -> 2.87 us  [local(): jnp.concatenate(lax.all_gather(tokens, 'tp'), axis=1).astype(jnp.float32)]
    dot_general x6, matrix products: 6.52 us -> 4.21 us  [local(): jnp.dot(scaled, weight, preferred_element_type=jnp.float32)]
    all_gather x1, blocking collectives: 31.3 us -> 33.3 us  [local(): value_piece = lax.all_gather(value, 'sp', axis=0, tiled=True)]
  transfers between devices with their start and end apart: 3 -> 3, of which waited for: 3 -> 2; matrix products, arithmetic and copies ran while one was open for 1% -> 9% of each run, Pallas kernels for 0% -> 0%
where the time goes in v1:
time: 200 us; the launch traced here: 199 us
  blocking collectives  72.7 us (36%)
  waiting for transfers between devices  66.5 us (33%)
  between operations  14.6 us (7%)
  local copies, waits for them, and re-layouts  14.1 us (7%)
  matrix products  12 us (6%)
  other arithmetic  9.77 us (5%)
  loops' own time  5.47 us (3%)
  starting transfers between devices  3.42 us (2%)
    reduce_scatter x1, waiting for transfers between devices, local(): lax.psum_scatter((jnp.dot(y_conv, out_conv, preferred_element_type=jnp.fl...  48 us
    all_gather x1, blocking collectives, local(): key_piece = lax.all_gather(key, 'sp', axis=0, tiled=True)  33.4 us
    all_gather x1, blocking collectives, local(): value_piece = lax.all_gather(value, 'sp', axis=0, tiled=True)  33.3 us
    all_gather x1, waiting for transfers between devices, local(): lax.all_gather(tokens, 'tp')  17.8 us
    psum x1, blocking collectives, local(): total_sq = lax.psum(jnp.sum(conv * conv, axis=1), 'tp')  5.98 us
    another operation x1, loops' own time, local(): lax.scan(visit, start_attn, (stacked_keys, stacked_values, firsts))  5.29 us
    dynamic_slice x8, local copies, waits for them, and re-layouts, local(): lax.scan(visit, start_attn, (stacked_keys, stacked_values, firsts))  5.18 us
    dot_general x6, matrix products, local(): jnp.dot(scaled, weight, preferred_element_type=jnp.float32)  4.21 us
  transfers between devices with their start and end apart: 3, of which 2 were waited for; matrix products, arithmetic and copies ran while one was open for 9% of the time, Pallas kernels for 0%

profile of v1, /device:TPU:0, one launch (start us, length us, event | category | flops | bytes accessed | tf_op | source)
XLA Modules:
  0.0 198.5 jit_solution(8787350900772154160)
XLA Ops:
  6.5 0.0 copy-start
  6.5 0.0 all-gather.3.cloned.1.call-start
  6.5 0.7 all-gather.3.cloned.1.call-update
  7.3 0.0 reduce-scatter.2.cloned.1.call-start
  7.3 0.5 slice.269
  7.8 0.7 convert_element_type.83
  8.5 0.7 convert_element_type.92
  9.9 0.7 slice_bitcast_fusion.33
  10.6 17.8 %all-gather.3.cloned.1.call-done = bf16[1024,512]{1,0:T(8,128)(2,1)} async-done(((bf16[256,512]{1,0:T(8,128)(2,1)}), bf16[1024,512]{1,0:T(8,128)(2,1)}) %all-gather.3.cloned.1.call-update) | async-done | bytes 1048592 | tf_op jit(solution)/shard_map/all_gather | solution.py:42
  28.3 1.5 fusion.18
  29.9 2.8 %convert_bitcast_fusion = f32[256,4,512]{2,0,1:T(8,128)} fusion(bf16[1024,512]{1,0:T(8,128)(2,1)} %all-gather.3.cloned.1.call-done), kind=kLoop, calls=%fused_computation.27 | loop fusion | flops 524288 | bytes 3145728 | tf_op jit(solution)/shard_map/convert_element_type | solution.py:42
  32.7 2.9 %copy.35 = f32[256,4,512]{0,2,1:T(8,128)} copy(f32[256,4,512]{2,0,1:T(8,128)} %convert_bitcast_fusion) | data formatting | bytes 4194304 | tf_op jit(solution)/shard_map/convert_element_type | solution.py:42
  35.6 2.0 %fusion.19 = bf16[256,2048]{0,1:T(8,128)(2,1)S(1)} fusion(f32[256,4,512]{0,2,1:T(8,128)} %copy.35, f32[2048]{0:T(1024)S(1)} %convert_element_type.83), kind=kLoop, calls=%fused_computation.31 | loop fusion | flops 1048576 | bytes 3153920 | tf_op jit(solution)/shard_map/convert_element_type | solution.py:44
  37.6 0.0 copy-done.2
  37.6 0.0 copy-start.25
  37.6 0.5 fusion.36
  38.1 0.0 copy-done.3
  38.1 0.0 copy-start.26
  38.1 0.5 fusion.35
  38.6 0.2 copy-done.25
  38.9 0.5 fusion.20
  39.4 0.0 copy-done.26
  39.4 0.5 fusion.32
  39.9 0.0 copy-done.1
  39.9 0.5 fusion.26
  40.4 3.4 %collective-permute-start = (bf16[30,128]{1,0:T(8,128)(2,1)S(1)}, bf16[30,128]{1,0:T(8,128)(2,1)S(1)}, u32[]{:S(2)}, u32[]{:S(2)}) collective-permute-start(bf16[30,128]{1,0:T(8,128)(2,1)S(1)} %slice.274), channel_id=1, source_target_pairs={{0,4},{4,8},{8,12},{12,16},{16,20},{20,24},{24,28},{1,5},{5,9},{9,... | collective-permute-start | bytes 23048 | tf_op jit(solution)/shard_map/ppermute | solution.py:20
  43.8 33.4 %all_gather.14 = bf16[2048,128]{1,0:T(8,128)(2,1)} all-gather(bf16[256,128]{1,0:T(8,128)(2,1)S(1)} %fusion.35), channel_id=1, replica_groups=mesh['sp'=8,'tp'=4] {'sp'}, dimensions={0}, use_global_device_ids=true | all-gather | bytes 589824 | tf_op jit(solution)/shard_map/all_gather | solution.py:81
  77.3 33.3 %all_gather.15 = bf16[2048,128]{1,0:T(8,128)(2,1)} all-gather(bf16[256,128]{1,0:T(8,128)(2,1)S(1)} %fusion.36), channel_id=1, replica_groups=mesh['sp'=8,'tp'=4] {'sp'}, dimensions={0}, use_global_device_ids=true | all-gather | bytes 589824 | tf_op jit(solution)/shard_map/all_gather | solution.py:82
  110.6 2.4 %reshape.167 = bf16[8,256,1,2,64]{4,3,1,0,2:T(2,128)(2,1)S(1)} reshape(bf16[2048,128]{1,0:T(8,128)(2,1)} %all_gather.14) | data formatting | bytes 1048576 | tf_op jit(solution)/shard_map/reshape | solution.py:84
  113.0 1.8 copy.37
  114.9 0.0 copy-start.24
  114.9 0.0 copy-start.22
  114.9 14.2 %while.17 = (s32[]{:T(128)}, f32[1,2,2,256]{3,1,2,0:T(2,128)S(1)}, f32[1,2,2,256]{3,1,2,0:T(2,128)S(1)}, f32[1,2,2,256,128]{4,3,2,1,0:T(8,128)S(1)}, s32[8]{0:T(...) while((s32[]{:T(128)}, f32[1,2,2,256]{3,1,2,0:T(2,128)S(1)}, ...), condition=%wide.region_8.9_spmd.clone, body=%wide.region_3.8_spmd.clone.sunk | while | flops 102567424 | bytes 4665639 | solution.py:126
  114.9 0.6 dynamic_slice.38
  116.2 3.6 %conditional.3 = ((f32[1,2,2,256]{3,1,2,0:T(2,128)S(1)}, f32[1,2,2,256]{3,1,2,0:T(2,128)S(1)}, f32[1,2,2,256,128]{4,3,2,1,0:T(8,128)S(1)})) conditional(s32[]{:T(128)} %convert_element_type.175, (f32[1,2,2,256]{3,1,2,0:T(2,128)S(1)}, f32[1,2,2,256]{3,1,2,0:T(2,128)S(1)}, f32[1,2,2,256,128]{4,3,2,1,0:T(8,128)S(1)}) %tuple.83, (s32[]{:T(128)}, ...), branch_computations={%region_4.4_spmd, %region_5.7_spmd} | conditional | flops 102567424 | bytes 4664360 | solution.py:123
  116.2 0.6 broadcast_add_fusion
  116.8 0.1 broadcast_compare_fusion
  116.9 1.2 fusion.86
  118.2 0.2 fusion.7
  118.4 1.4 fusion.4
  119.8 0.6 dynamic_slice.38
  121.1 0.6 dynamic_slice.38
  122.5 0.6 dynamic_slice.38
  123.8 0.6 dynamic_slice.38
  125.1 0.6 dynamic_slice.38
  126.4 0.6 dynamic_slice.38
  127.8 0.6 dynamic_slice.38
  129.1 0.3 multiply_reduce_fusion
  129.5 0.1 multiply_bitcast_fusion
  129.6 0.1 copy.41
  129.7 0.0 copy-start.6
  129.9 1.8 fusion.40
  131.7 0.0 collective-permute-done
  131.9 0.0 copy-start.4
  131.9 0.0 copy-start.5
  131.9 0.0 copy-start.23
  131.9 0.6 multiply_reduce_fusion.1
  132.5 6.0 %psum.7 = f32[256]{0:T(256)S(1)} all-reduce(f32[256]{0:T(256)S(1)} %get-tuple-element.297), channel_id=1, replica_groups=mesh['sp'=8,'tp'=4] {'tp'}, use_global_device_ids=true, to_apply=%region_2.3 | all-reduce | flops 256 | bytes 2048 | tf_op jit(solution)/shard_map/psum | solution.py:145
  138.5 0.0 copy-done.4
  138.5 2.2 %fusion.71 = f32[256,2048]{1,0:T(8,128)} fusion(bf16[128,2048]{1,0:T(8,128)(2,1)S(1)} %copy-done.4, bf16[256,2048]{0,1:T(8,128)(2,1)S(1)} %fusion.19, bf16[2048,128]{1,0:T(8,128)(2,1)S(1)} %copy-done.5, f32[256,128]{1,0:T(8,128)S(1)} %get-tuple-element.298, f32[128]{0:T(128)S(1)} %copy-done.23, f32[256]{0:T(256)S(1)} %add_rsqrt_fusion.1, ...), kind=kOutput, calls=%fused_computation.127 | convolution fusion | flops 268926976 | bytes 4327936 | tf_op jit(solution)/shard_map/dot_general | solution.py:150
  140.6 0.0 copy-done
  140.6 3.0 %fusion.17 = bf16[256,2048]{1,0:T(8,128)(2,1)} fusion(f32[256,2048]{1,0:T(8,128)} %fusion.71, bf16[256,256]{0,1:T(8,128)(2,1)S(1)} %fusion.40, bf16[256,2048]{1,0:T(8,128)(2,1)S(1)} %copy-done), kind=kOutput, calls=%fused_computation.28 | convolution fusion | flops 269484032 | bytes 4325376 | tf_op jit(solution)/shard_map/dot_general | solution.py:151
  143.7 0.0 reduce-scatter.2.cloned.1.call-update
  143.7 48.0 %reduce-scatter.2.cloned.1.call-done = bf16[64,2048]{1,0:T(8,128)(2,1)} async-done(((bf16[256,2048]{1,0:T(8,128)(2,1)}), bf16[64,2048]{1,0:T(8,128)(2,1)}) %reduce-scatter.2.cloned.1.call-update) | async-done | bytes 262160 | tf_op jit(solution)/shard_map/reduce_scatter | solution.py:148
  (70 shorter events, 0.4 us)
Async XLA Ops:
  6.5 134.1 %copy-start = (bf16[256,2048]{1,0:T(8,128)(2,1)S(1)}, bf16[256,2048]{1,0:T(8,128)(2,1)}, u32[]{:S(2)}) copy-start(bf16[256,2048]{1,0:T(8,128)(2,1)} %param.33) | copy-start | bytes 3145732
  6.5 21.8 %all-gather.3.cloned.1.call-start = ((), (), s32[]{:S(2)}) async-start(), calls=%async_computation.2 | async-start | bytes 1310720 | tf_op jit(solution)/shard_map/all_gather | solution.py:42
  7.3 184.4 %reduce-scatter.2.cloned.1.call-start = ((), (), s32[]{:S(2)}) async-start(), calls=%async_computation.1 | async-start | bytes 1310720 | tf_op jit(solution)/shard_map/reduce_scatter | solution.py:148
  35.6 2.0 %copy-start.2 = (bf16[2048,128]{1,0:T(8,128)(2,1)S(1)}, bf16[2048,128]{1,0:T(8,128)(2,1)}, u32[]{:S(2)}) copy-start(bf16[2048,128]{1,0:T(8,128)(2,1)} %param.25) | copy-start | bytes 1572868
  35.6 2.5 %copy-start.3 = (bf16[2048,128]{1,0:T(8,128)(2,1)S(1)}, bf16[2048,128]{1,0:T(8,128)(2,1)}, u32[]{:S(2)}) copy-start(bf16[2048,128]{1,0:T(8,128)(2,1)} %param.24) | copy-start | bytes 1572868
  37.6 1.2 copy-start.25
  38.1 1.3 copy-start.26
  38.8 1.1 copy-start.1
  40.4 91.3 %collective-permute-start = (bf16[30,128]{1,0:T(8,128)(2,1)S(1)}, bf16[30,128]{1,0:T(8,128)(2,1)S(1)}, u32[]{:S(2)}, u32[]{:S(2)}) collective-permute-start(bf16[30,128]{1,0:T(8,128)(2,1)S(1)} %slice.274), channel_id=1, source_target_pairs={{0,4},{4,8},{8,12},{12,16},{16,20},{20,24},{24,28},{1,5},{5,9},{9,... | collective-permute-start | bytes 23048 | tf_op jit(solution)/shard_map/ppermute | solution.py:20
  114.9 14.2 %copy-start.24 = (f32[2]{0:T(128)S(1)}, f32[2]{0:T(128)}, u32[]{:S(2)}) copy-start(f32[2]{0:T(128)} %param.30) | copy-start | bytes 28
  114.9 14.6 %copy-start.22 = (f32[128]{0:T(128)S(1)}, f32[128]{0:T(128)}, u32[]{:S(2)}) copy-start(f32[128]{0:T(128)} %param.31) | copy-start | bytes 1540
  129.7 2.0 copy-start.6
  129.7 2.0 copy-start.7
  129.8 2.0 copy-start.8
  129.8 2.0 copy-start.9
  129.8 2.0 copy-start.10
  129.8 2.0 copy-start.11
  129.8 2.0 copy-start.12
  129.8 2.0 copy-start.13
  129.8 2.0 copy-start.14
  129.8 2.0 copy-start.15
  129.8 2.0 copy-start.16
  129.8 2.0 copy-start.17
  129.9 2.0 copy-start.18
  129.9 2.0 copy-start.19
  129.9 2.0 copy-start.20
  129.9 2.0 copy-start.21
  131.9 6.6 %copy-start.4 = (bf16[128,2048]{1,0:T(8,128)(2,1)S(1)}, bf16[128,2048]{1,0:T(8,128)(2,1)}, u32[]{:S(2)}) copy-start(bf16[128,2048]{1,0:T(8,128)(2,1)} %param.32) | copy-start | bytes 1572868
  131.9 6.6 %copy-start.5 = (bf16[2048,128]{1,0:T(8,128)(2,1)S(1)}, bf16[2048,128]{1,0:T(8,128)(2,1)}, u32[]{:S(2)}) copy-start(bf16[2048,128]{1,0:T(8,128)(2,1)} %param.26) | copy-start | bytes 1572868
  131.9 6.6 %copy-start.23 = (f32[128]{0:T(128)S(1)}, f32[128]{0:T(128)}, u32[]{:S(2)}) copy-start(f32[128]{0:T(128)} %param.29) | copy-start | bytes 1540
Sparse Core Ops, SparseCore 0:
  8.9 19.4 all-gather.2
  143.8 47.8 reduce-scatter.1
